TPU v7x, 32 devices: a whole 2x2x4 slice. The times are simulated.
32 devices in a mesh: fs: 8 (over z, x), tp: 4 (over y, core).
Axes of the slice: x: 2, y: 2, z: 4, core: 2. Of those that a mesh axis runs over, the one named last changes fastest.
Arguments:
- prompt_tokens: bfloat16 [6144, 2048], P('fs', 'tp'), may hold values from -6 to 6
- norm_gain: float32 [2048], P('fs'), may hold values from 0.1 to 1.9
- up_master: float32 [2048, 4096], P('fs', 'tp'), may hold values from -6 to 6
- down_master: float32 [2048, 4096], P('fs', 'tp'), may hold values from -6 to 6
Outputs:
- serve_up: bfloat16 [2048, 4096], P(None, 'tp')
- serve_down: bfloat16 [2048, 4096], P(None, 'tp')
- mixed: bfloat16 [6144, 2048], P('fs', 'tp')
All inputs are finite; a program needn't handle non-finite values.
Results may differ from a plain program's by a relative error of at most 0.009.
Values may be sent and summed in bfloat16 or wider, within the bound.
A program may use at most 64 MiB of HBM per device.

v0:
```python
import jax
import jax.numpy as jnp
from jax import lax
from jax.sharding import PartitionSpec as P


def shards(prompt_tokens, norm_gain, up_master, down_master):
    up_folded = (norm_gain[:, None] * up_master).astype(jnp.bfloat16)
    down_cast = down_master.astype(jnp.bfloat16)
    whole = lax.all_gather(prompt_tokens, "tp", axis=1, tiled=True)
    width = whole.shape[1]
    hidden_units = up_master.shape[1] * lax.axis_size("tp")
    wide = whole.astype(jnp.float32)
    normed = (wide * lax.rsqrt(jnp.mean(wide * wide, axis=1, keepdims=True) + 1e-05)).astype(
        jnp.bfloat16
    )
    contract = (((1,), (1,)), ((), ()))
    serve_up, serve_down = (
        lax.all_gather(up_folded, "fs", axis=0, tiled=True),
        lax.all_gather(down_cast, "fs", axis=0, tiled=True),
    )
    hidden = jnp.dot(normed, serve_up, preferred_element_type=jnp.float32)
    act = jnp.square(jax.nn.relu(hidden * width ** (-0.5))).astype(jnp.bfloat16)
    product = lax.dot_general(act, serve_down, contract, preferred_element_type=jnp.float32)
    partial_value = (product * hidden_units ** (-0.5)).astype(jnp.bfloat16).astype(jnp.float32)
    mixed = lax.psum_scatter(
        partial_value.astype(jnp.bfloat16), "tp", scatter_dimension=1, tiled=True
    )
    return (serve_up, serve_down, mixed)


def solution(mesh):
    return jax.shard_map(
        shards,
        mesh=mesh,
        in_specs=(P("fs", "tp"), P("fs"), P("fs", "tp"), P("fs", "tp")),
        out_specs=(P(None, "tp"), P(None, "tp"), P("fs", "tp")),
        check_vma=False,
    )
```

profile of v0, /device:TPU:7, one launch (start us, length us, event | category | flops | bytes accessed | tf_op | source)
XLA Modules:
  0.0 249.7 jit_solution(355867088768193261)
XLA Ops:
  7.2 0.0 all-gather.8.cloned.1.call-start
  7.2 0.7 all-gather.8.cloned.1.call-update
  7.9 0.0 all-gather.4.cloned.1.call-start
  7.9 2.1 multiply_convert_fusion.2
  10.1 0.0 all-gather.4.cloned.1.call-update
  10.1 0.0 all-gather.6.cloned.1.call-start
  10.2 2.1 convert_element_type.21
  12.3 0.0 all-gather.6.cloned.1.call-update
  12.3 0.0 reduce-scatter.2.cloned.1.call-start
  12.3 26.4 %all-gather.8.cloned.1.call-done = bf16[768,2048]{1,0:T(8,128)(2,1)} async-done(((bf16[768,512]{1,0:T(8,128)(2,1)}), bf16[768,2048]{1,0:T(8,128)(2,1)}) %all-gather.8.cloned.1.call-update) | async-done | bytes 3145744 | tf_op jit(solution)/shard_map/all_gather | solution.py:10
  38.7 2.6 %fusion = f32[768]{0:T(1024)S(1)} fusion(bf16[768,2048]{1,0:T(8,128)(2,1)} %all-gather.8.cloned.1.call-done), kind=kLoop, calls=%fused_computation.2 | loop fusion | flops 4717824 | bytes 3148800 | tf_op jit(solution)/shard_map/reduce_sum | solution.py:14
  41.3 71.3 %all-gather.4.cloned.1.call-done = bf16[2048,1024]{1,0:T(8,128)(2,1)} async-done(((bf16[256,1024]{1,0:T(8,128)(2,1)}), bf16[2048,1024]{1,0:T(8,128)(2,1)}) %all-gather.4.cloned.1.call-update) | async-done | bytes 4194320 | tf_op jit(solution)/shard_map/all_gather | solution.py:19
  112.6 74.1 %all-gather.6.cloned.1.call-done = bf16[2048,1024]{1,0:T(8,128)(2,1)} async-done(((bf16[256,1024]{1,0:T(8,128)(2,1)}), bf16[2048,1024]{1,0:T(8,128)(2,1)}) %all-gather.6.cloned.1.call-update) | async-done | bytes 4194320 | tf_op jit(solution)/shard_map/all_gather | solution.py:20
  186.7 12.1 %multiply_convert_fusion = bf16[768,2048]{1,0:T(8,128)(2,1)} fusion(bf16[2048,1024]{1,0:T(8,128)(2,1)} %all-gather.6.cloned.1.call-done, bf16[2048,1024]{1,0:T(8,128)(2,1)} %all-gather.4.cloned.1.call-done, bf16[768,2048]{1,0:T(8,128)(2,1)} %all-gather.8.cloned.1.call-done, f32[768]{0:T(1024)S(1)} %add_rsqrt_fusion), kind=kOutput, calls=%fused_computation.4 | convolution fusion | flops 6453460992 | bytes 14683136 | tf_op jit(solution)/shard_map/dot_general | solution.py:24
  198.8 0.0 reduce-scatter.2.cloned.1.call-update
  198.9 37.5 %reduce-scatter.2.cloned.1.call-done = bf16[768,512]{1,0:T(8,128)(2,1)} async-done(((bf16[768,2048]{1,0:T(8,128)(2,1)}), bf16[768,512]{1,0:T(8,128)(2,1)}) %reduce-scatter.2.cloned.1.call-update) | async-done | bytes 786448 | tf_op jit(solution)/shard_map/reduce_scatter | solution.py:26
  236.3 0.0 copy-start
  236.3 4.8 %copy.9 = bf16[2048,1024]{1,0:T(8,128)(2,1)} copy(bf16[2048,1024]{1,0:T(8,128)(2,1)} %all-gather.4.cloned.1.call-done) | data formatting | bytes 8388608
  241.1 0.0 copy-done
  241.1 2.0 copy.10
  (1 shorter events, 0.0 us)
Async XLA Ops:
  7.2 31.6 %all-gather.8.cloned.1.call-start = ((), (), s32[]{:S(2)}) async-start(), calls=%async_computation.3 | async-start | bytes 3932160 | tf_op jit(solution)/shard_map/all_gather | solution.py:10
  7.9 104.8 %all-gather.4.cloned.1.call-start = ((), (), s32[]{:S(2)}) async-start(), calls=%async_computation.1 | async-start | bytes 4718592 | tf_op jit(solution)/shard_map/all_gather | solution.py:19
  10.1 176.6 %all-gather.6.cloned.1.call-start = ((), (), s32[]{:S(2)}) async-start(), calls=%async_computation.2 | async-start | bytes 4718592 | tf_op jit(solution)/shard_map/all_gather | solution.py:20
  12.3 224.0 %reduce-scatter.2.cloned.1.call-start = ((), (), s32[]{:S(2)}) async-start(), calls=%async_computation.4 | async-start | bytes 3932160 | tf_op jit(solution)/shard_map/reduce_scatter | solution.py:26
  236.3 4.8 %copy-start = (bf16[2048,1024]{1,0:T(8,128)(2,1)S(1)}, bf16[2048,1024]{1,0:T(8,128)(2,1)}, u32[]{:S(2)}) copy-start(bf16[2048,1024]{1,0:T(8,128)(2,1)} %all-gather.6.cloned.1.call-done) | copy-start | bytes 12582916
Sparse Core Ops, SparseCore 0:
  9.5 29.1 all-gather.7
  41.4 71.1 all-gather.3
  115.4 71.3 all-gather.5
  199.0 37.2 reduce-scatter.1
where the time goes:
time: 253 us; the launch traced here: 250 us
  waiting for transfers between devices  210 us (83%)
  between operations  13.8 us (5%)
  matrix products  12.1 us (5%)
  local copies, waits for them, and re-layouts  6.83 us (3%)
  other arithmetic  6.82 us (3%)
    all_gather x1, waiting for transfers between devices, shards(): lax.all_gather(down_cast, 'fs', axis=0, tiled=True)  74.1 us
    all_gather x1, waiting for transfers between devices, shards(): lax.all_gather(up_folded, 'fs', axis=0, tiled=True)  71.3 us
    reduce_scatter x1, waiting for transfers between devices, shards(): lax.psum_scatter(partial_value.astype(jnp.bfloat16), 'tp', scatter_dimens...  37.5 us
    all_gather x1, waiting for transfers between devices, shards(): whole = lax.all_gather(prompt_tokens, 'tp', axis=1, tiled=True)  26.4 us
    dot_general x1, matrix products, shards(): lax.dot_general(act, serve_down, contract, preferred_element_type=jnp.flo...  12.1 us
    unnamed x4, local copies, waits for them, and re-layouts  6.83 us
  transfers between devices with their start and end apart: 4, of which 4 were waited for; matrix products, arithmetic and copies ran while one was open for 3% of the time, Pallas kernels for 0%

commit v1 on v0

v1 whole, which is shorter than its diff:
```python
import functools

import jax
import jax.numpy as jnp
from jax import lax
from jax.experimental import pallas as pl
from jax.experimental.pallas import tpu as pltpu
from jax.sharding import PartitionSpec as P

MESH = pl.DeviceIdType.MESH
LANES = 128


def plain(prompt_tokens, norm_gain, up_master, down_master):
    up_folded = (norm_gain[:, None] * up_master).astype(jnp.bfloat16)
    down_cast = down_master.astype(jnp.bfloat16)
    whole = lax.all_gather(prompt_tokens, "tp", axis=1, tiled=True)
    width = whole.shape[1]
    hidden_units = up_master.shape[1] * lax.axis_size("tp")
    wide = whole.astype(jnp.float32)
    normed = (wide * lax.rsqrt(jnp.mean(wide * wide, axis=1, keepdims=True) + 1e-05)).astype(
        jnp.bfloat16
    )
    contract = (((1,), (1,)), ((), ()))
    serve_up, serve_down = (
        lax.all_gather(up_folded, "fs", axis=0, tiled=True),
        lax.all_gather(down_cast, "fs", axis=0, tiled=True),
    )
    hidden = jnp.dot(normed, serve_up, preferred_element_type=jnp.float32)
    act = jnp.square(jax.nn.relu(hidden * width ** (-0.5))).astype(jnp.bfloat16)
    product = lax.dot_general(act, serve_down, contract, preferred_element_type=jnp.float32)
    partial_value = (product * hidden_units ** (-0.5)).astype(jnp.bfloat16)
    mixed = lax.psum_scatter(partial_value, "tp", scatter_dimension=1, tiled=True)
    return (serve_up, serve_down, mixed)


def kernel(line, pieces, tok, gain, up, down, out_up, out_down, mixed,
           wu, wd, xt, xn, act, part, pbuf, psum, rin_p, rin_y,
           w_send, w_recv, t_send, t_recv, a_send, a_recv, b_send, b_recv, c_send, c_recv,
           o_sem, l_sem):
    T, dl = tok.shape
    r, F = up.shape
    D = wu.shape[0]
    tp = lax.axis_index("tp")
    fs = lax.axis_index("fs")
    z, x = fs // 2, fs % 2
    core, chip = tp % 2, tp // 2
    partner = tp + 1 - 2 * core
    mirror = (tp + 2) % 4
    diag = (partner + 2) % 4
    has_up, has_dn = z < line - 1, z > 0
    W = (wu, wd)
    nb = dl // LANES
    per = r // LANES
    half = T // 2
    zdev = ((fs + 2, tp), (fs - 2, tp), (fs + 1 - 2 * x, tp))

    barrier = pltpu.get_barrier_semaphore()

    def greet(dev):
        pl.semaphore_signal(barrier, inc=1, device_id=dev, device_id_type=MESH)

    for other in (partner, mirror, diag):
        greet((fs, other))
    greet(zdev[2])
    pl.when(has_up)(lambda: greet(zdev[0]))
    pl.when(has_dn)(lambda: greet(zdev[1]))

    base = pl.multiple_of(fs * r, r)
    for i in range(r // LANES):
        rows = slice(i * LANES, (i + 1) * LANES)
        g = jnp.transpose(jnp.broadcast_to(gain[:, rows], (LANES, LANES)))
        for c in range(F // LANES):
            cols = slice(c * LANES, (c + 1) * LANES)
            wu[pl.ds(base + i * LANES, LANES), cols] = (g * up[rows, cols]).astype(jnp.bfloat16)
    wd[pl.ds(base, r), :] = down[...].astype(jnp.bfloat16)
    own_tok = pltpu.make_async_copy(tok, xt.at[tp], l_sem)
    own_tok.start()
    links = 4 + has_up.astype(jnp.int32) + has_dn.astype(jnp.int32)
    pl.semaphore_wait(barrier, links)

    def piece(a, s, p, way):
        start, size = pieces[p][0], pieces[p][1]
        ref = W[a].at[pl.ds(pl.multiple_of(s * r + start, 16), size), :]
        return pltpu.make_async_remote_copy(
            src_ref=ref, dst_ref=ref, send_sem=w_send.at[way, a, s, p],
            recv_sem=w_recv.at[a, s, p], device_id=zdev[way], device_id_type=MESH)

    def tok_copy(src, k, slot, to):
        return pltpu.make_async_remote_copy(
            src_ref=src, dst_ref=xt.at[k], send_sem=t_send.at[slot], recv_sem=t_recv.at[k],
            device_id=(fs, to), device_id_type=MESH)

    one = [p for p in range(len(pieces)) if pieces[p][2] == 1]
    two = [p for p in range(len(pieces)) if pieces[p][2] == 2]

    def start(d):
        d.start()

    def wait_send(d):
        d.wait_send()

    def own_z(a, do):
        for p in one + two:
            pl.when(has_up)(lambda: do(piece(a, fs, p, 0)))
            pl.when(has_dn)(lambda: do(piece(a, fs, p, 1)))

    def own_x(a, do):
        for p in two + one:
            do(piece(a, fs, p, 2))

    xs = fs + 1 - 2 * x

    def cross(a, do, wait):
        for p in two:
            if wait:
                piece(a, xs, p, 2).wait_recv()
            pl.when(has_up)(lambda: do(piece(a, xs, p, 0)))
            pl.when(has_dn)(lambda: do(piece(a, xs, p, 1)))

    def place(idx):
        got = jnp.int32(0)
        for i in range(line):
            order = sorted(range(line), key=lambda k: (abs(k - i), k if i < line / 2 else -k))
            for q in range(line):
                got = got + jnp.where((z == i) & (idx == q), jnp.int32(order[q]), jnp.int32(0))
        return got

    def relay(a, idx, do, wait):
        zz = place(idx)
        onward_up = (zz < z) & has_up
        onward_dn = (zz > z) & has_dn
        same, cross_s = zz * 2 + x, zz * 2 + 1 - x
        for p in one:
            if wait:
                piece(a, same, p, 2).wait_recv()
            pl.when(onward_up)(lambda: do(piece(a, same, p, 0)))
            pl.when(onward_dn)(lambda: do(piece(a, same, p, 1)))
            do(piece(a, same, p, 2))
        for p in two:
            for s in (same, cross_s):
                if wait:
                    piece(a, s, p, 2).wait_recv()
                pl.when(onward_up)(lambda: do(piece(a, s, p, 0)))
                pl.when(onward_dn)(lambda: do(piece(a, s, p, 1)))

    tok_copy(tok, tp, 0, mirror).start()
    own_x(0, start)
    own_z(0, start)
    tok_copy(tok, tp, 1, partner).start()
    cross(0, start, True)
    for idx in range(1, line):
        relay(0, jnp.int32(idx), start, True)
        if idx == 1:
            tok_copy(tok, mirror, 0, mirror).wait_recv()
            tok_copy(xt.at[mirror], mirror, 2, partner).start()
    own_z(1, start)
    own_x(1, start)

    own_tok.wait()
    tok_copy(tok, partner, 1, partner).wait_recv()
    tok_copy(tok, diag, 1, partner).wait_recv()
    block = 64

    def norm(i, carry):
        rows = pl.ds(pl.multiple_of(i * block, block), block)
        wide = [xt[k, rows, :].astype(jnp.float32) for k in range(4)]
        sq = wide[0] * wide[0]
        for k in range(1, 4):
            sq = sq + wide[k] * wide[k]
        inv = lax.rsqrt(jnp.sum(sq, axis=1, keepdims=True) * (1.0 / D) + 1e-05)
        for k in range(4):
            xn[rows, k * dl:(k + 1) * dl] = (wide[k] * inv).astype(jnp.bfloat16)
        return carry

    lax.fori_loop(0, T // block, norm, 0)

    cross(1, start, True)
    for idx in range(line):
        s = place(jnp.int32(idx)) * 2 + 1 - x
        for p in one:
            piece(0, s, p, 2).wait_recv()
    up_out = pltpu.make_async_copy(wu, out_up, o_sem.at[line])
    up_out.start()

    mrows = LANES

    def first(i, carry):
        rows = pl.ds(pl.multiple_of(i * mrows, mrows), mrows)
        hidden = jnp.dot(xn[rows, :], wu[...], preferred_element_type=jnp.float32) * D ** (-0.5)
        hidden = jnp.maximum(hidden, 0.0)
        act[rows, :] = (hidden * hidden).astype(jnp.bfloat16)
        return carry

    lax.fori_loop(0, T // mrows, first, 0)
    relay(1, jnp.int32(1), start, True)

    scale = (F * 4) ** (-0.5)
    mine = pl.ds(pl.multiple_of(core * half, half), half)
    theirs = pl.ds(pl.multiple_of((1 - core) * half, half), half)
    steps = 2 * per

    def block_of(n):
        zz, j = place(n // steps), n % steps
        side = j // per
        s = zz * 2 + x + side * (1 - 2 * x)
        return s * per + j % per

    def owner_of(b):
        o = b // nb
        return o, (o // 2) == chip

    def to_partner(b):
        return pltpu.make_async_remote_copy(
            src_ref=part.at[b], dst_ref=rin_p.at[b % nb], send_sem=a_send.at[b],
            recv_sem=a_recv.at[b % nb], device_id=(fs, partner), device_id_type=MESH)

    def swap(b):
        return pltpu.make_async_remote_copy(
            src_ref=part.at[b, theirs, :], dst_ref=pbuf.at[b], send_sem=b_send.at[b],
            recv_sem=b_recv.at[b], device_id=(fs, partner), device_id_type=MESH)

    def to_owner(b, o):
        return pltpu.make_async_remote_copy(
            src_ref=psum.at[b], dst_ref=rin_y.at[b % nb, mine, :], send_sem=c_send.at[b],
            recv_sem=c_recv.at[b % nb, core], device_id=(fs, o), device_id_type=MESH)

    def second_half(b):
        o, here = owner_of(b)

        @pl.when(jnp.logical_not(here))
        def _():
            swap(b).wait_recv()
            psum[b] = (part[b, mine, :].astype(jnp.float32)
                       + pbuf[b].astype(jnp.float32)).astype(jnp.bfloat16)
            to_owner(b, o).start()

    def out_copy(idx):
        rows = pl.ds(pl.multiple_of(place(idx) * 2 * r, 2 * r), 2 * r)
        return pltpu.make_async_copy(wd.at[rows, :], out_down.at[rows, :], o_sem.at[idx])

    def body(n, carry):
        idx, j = n // steps, n % steps

        @pl.when((j == 0) & (idx >= 1) & (idx + 1 < line))
        def _():
            relay(1, idx + 1, start, True)

        far = place(idx) * 2 + 1 - x
        for h in range(per):
            @pl.when(j == per + h)
            def _():
                for p in one:
                    if pieces[p][0] // LANES == h:
                        piece(1, far, p, 2).wait_recv()
        b = block_of(n)
        rhs = wd[pl.ds(pl.multiple_of(b * LANES, LANES), LANES), :]
        product = lax.dot_general(act[...], rhs, (((1,), (1,)), ((), ())),
                                  preferred_element_type=jnp.float32)
        part[b] = (product * scale).astype(jnp.bfloat16)
        o, here = owner_of(b)

        @pl.when(here & (o != tp))
        def _():
            to_partner(b).start()

        @pl.when(jnp.logical_not(here))
        def _():
            swap(b).start()

        @pl.when(j == steps - 1)
        def _():
            out_copy(idx).start()

        @pl.when(n > 0)
        def _():
            second_half(block_of(n - 1))

        return carry

    total = line * steps
    lax.fori_loop(0, total, body, 0)
    second_half(block_of(jnp.int32(total - 1)))

    for i in range(nb):
        b = tp * nb + i
        to_partner(b).wait_recv()
        for c in range(2):
            pltpu.make_async_remote_copy(
                src_ref=psum.at[b], dst_ref=rin_y.at[i, c * half:(c + 1) * half, :],
                send_sem=c_send.at[b], recv_sem=c_recv.at[i, c],
                device_id=(fs, partner), device_id_type=MESH).wait_recv()
        mixed[:, i * LANES:(i + 1) * LANES] = (
            part[b].astype(jnp.float32) + rin_p[i].astype(jnp.float32)
            + rin_y[i].astype(jnp.float32)).astype(jnp.bfloat16)

    for slot, (k, to) in enumerate(((tp, mirror), (tp, partner), (mirror, partner))):
        tok_copy(xt.at[k], k, slot, to).wait_send()
    for a in range(2):
        own_x(a, wait_send)
        own_z(a, wait_send)
        cross(a, wait_send, False)

    def drain(idx, carry):
        for a in range(2):
            relay(a, idx, wait_send, False)
        return carry

    lax.fori_loop(1, line, drain, 0)

    def drain_sums(b, carry):
        o, here = owner_of(b)

        @pl.when(here & (o != tp))
        def _():
            to_partner(b).wait_send()

        @pl.when(jnp.logical_not(here))
        def _():
            swap(b).wait_send()
            to_owner(b, o).wait_send()

        return carry

    lax.fori_loop(0, D // LANES, drain_sums, 0)
    up_out.wait()

    def drain_out(idx, carry):
        out_copy(idx).wait()
        return carry

    lax.fori_loop(0, line, drain_out, 0)


def cut(r):
    across = min(LANES - 16, max(16, (r * 3 // 16) // 16 * 16))
    got = []
    for first in range(0, r, LANES):
        rows = LANES if first + LANES < r else LANES - across
        if rows == LANES:
            got += [(first, LANES // 2, 1), (first + LANES // 2, LANES // 2, 1)]
        else:
            got += [(first, rows, 1)]
    return got + [(r - across, across, 2)]


def fused(n_fs, prompt_tokens, norm_gain, up_master, down_master):
    T, dl = prompt_tokens.shape
    r, F = up_master.shape
    D = r * n_fs
    line = n_fs // 2
    pieces = cut(r)
    nblk, nb, half = D // LANES, dl // LANES, T // 2
    bf = jnp.bfloat16
    dma = pltpu.SemaphoreType.DMA
    vmem = pl.BlockSpec(memory_space=pltpu.VMEM)
    hbm = pl.BlockSpec(memory_space=pl.ANY)
    return pl.pallas_call(
        functools.partial(kernel, line, pieces),
        out_shape=(jax.ShapeDtypeStruct((D, F), bf), jax.ShapeDtypeStruct((D, F), bf),
                   jax.ShapeDtypeStruct((T, dl), bf)),
        in_specs=[vmem] * 4,
        out_specs=(hbm, hbm, vmem),
        scratch_shapes=[
            pltpu.VMEM((D, F), bf), pltpu.VMEM((D, F), bf),
            pltpu.VMEM((4, T, dl), bf), pltpu.VMEM((T, D), bf), pltpu.VMEM((T, F), bf),
            pltpu.VMEM((nblk, T, LANES), bf), pltpu.VMEM((nblk, half, LANES), bf),
            pltpu.VMEM((nblk, half, LANES), bf),
            pltpu.VMEM((nb, T, LANES), bf), pltpu.VMEM((nb, T, LANES), bf),
            dma((3, 2, n_fs, len(pieces))), dma((2, n_fs, len(pieces))),
            dma((3,)), dma((4,)),
            dma((nblk,)), dma((nb,)), dma((nblk,)), dma((nblk,)), dma((nblk,)), dma((nb, 2)),
            dma((line + 1,)), dma,
        ],
        compiler_params=pltpu.CompilerParams(
            collective_id=0, has_side_effects=True, vmem_limit_bytes=56 * 2 ** 20),
    )(prompt_tokens, norm_gain.reshape(1, r), up_master, down_master)


def solution(mesh):
    n_fs, n_tp = mesh.shape["fs"], mesh.shape["tp"]

    def shards(prompt_tokens, norm_gain, up_master, down_master):
        T, dl = prompt_tokens.shape
        r = up_master.shape[0]
        fits = (n_tp == 4 and n_fs % 2 == 0 and n_fs >= 6 and r % LANES == 0
                and dl % LANES == 0 and T % (2 * LANES) == 0 and r * n_fs == dl * n_tp)
        if not fits:
            return plain(prompt_tokens, norm_gain, up_master, down_master)
        return fused(n_fs, prompt_tokens, norm_gain, up_master, down_master)

    return jax.shard_map(
        shards,
        mesh=mesh,
        in_specs=(P("fs", "tp"), P("fs"), P("fs", "tp"), P("fs", "tp")),
        out_specs=(P(None, "tp"), P(None, "tp"), P("fs", "tp")),
        check_vma=False,
    )
```

time: 253 us -> 126 us (0.50)
  waiting for transfers between devices: 210 us -> 0 us
  Pallas kernels: 0 us -> 116 us
  between operations: 13.8 us -> 0.65 us
  matrix products: 12.1 us -> 0 us
  other arithmetic: 6.82 us -> 0 us
    all_gather x3 -> x0, waiting for transfers between devices: 172 us -> none  [the longest x1 74.1 us: shards(): lax.all_gather(down_cast, 'fs', axis=0, tiled=True)]
    pallas_call x0 -> x1, Pallas kernels: none -> 116 us  [fused(): pl.pallas_call(functools.partial(kernel, line, pieces), out_shape=(jax.Sh...]
    reduce_scatter x1 -> x0, waiting for transfers between devices: 37.5 us -> none  [shards(): lax.psum_scatter(partial_value.astype(jnp.bfloat16), 'tp', scatter_dimens...]
    dot_general x1 -> x0, matrix products: 12.1 us -> none  [shards(): lax.dot_general(act, serve_down, contract, preferred_element_type=jnp.flo...]
    convert_element_type x2 -> x0, other arithmetic: 4.24 us -> none  [the longest x1 2.14 us: shards(): up_folded = (norm_gain[:, None] * up_master).astype(jnp.bfloat16)]
    reduce_sum x1 -> x0, other arithmetic: 2.57 us -> none  [shards(): jnp.mean(wide * wide, axis=1, keepdims=True) + 1e-05]
    unnamed x4 -> x7, local copies, waits for them, and re-layouts: 6.83 us -> 7.72 us
  transfers between devices with their start and end apart: 4 -> 0, of which waited for: 4 -> 0; matrix products, arithmetic and copies ran while one was open for 3% -> 0% of each run, Pallas kernels for 0% -> 0%
where the time goes in v1:
time: 126 us; the launch traced here: 124 us
  Pallas kernels  116 us (92%)
  local copies, waits for them, and re-layouts  7.72 us (6%)
    pallas_call x1, Pallas kernels, fused(): pl.pallas_call(functools.partial(kernel, line, pieces), out_shape=(jax.Sh...  116 us
    unnamed x7, local copies, waits for them, and re-layouts  7.72 us

profile of v1, /device:TPU:7, one launch (start us, length us, event | category | flops | bytes accessed | tf_op | source)
XLA Modules:
  0.0 124.5 jit_solution(3999091523768297863)
XLA Ops:
  0.6 116.1 %shard_map.67 = (bf16[2048,1024]{1,0:T(8,128)(2,1)}, bf16[2048,1024]{1,0:T(8,128)(2,1)}, bf16[768,512]{1,0:T(8,128)(2,1)}) custom-call(bf16[768,512]{1,0:T(8,128)(2,1)} %tok.1, f32[1,256]{1,0:T(1,128)} %bitcast.1, f32[256,1024]{1,0:T(8,128)} %up.1, f32[256,1024]{1,0:T(8,128)} %down.1), custom_call_target="tpu_custom_call" | custom-call | tf_op jit(solution)/shard_map/pallas_call | solution.py:358
  116.8 0.0 copy-start
  116.8 4.8 %copy.10 = bf16[2048,1024]{1,0:T(8,128)(2,1)} copy(bf16[2048,1024]{1,0:T(8,128)(2,1)} %get-tuple-element.6) | data formatting | bytes 8388608
  121.6 0.0 copy-done
  121.6 0.0 copy-start.1
  121.6 2.0 %copy.11 = bf16[2048,1024]{1,0:T(8,128)(2,1)} copy(bf16[2048,1024]{1,0:T(8,128)(2,1)S(1)} %copy-done) | data formatting | bytes 8388608
  123.6 0.0 copy-done.1
  123.6 0.9 copy.12
Async XLA Ops:
  116.8 4.8 %copy-start = (bf16[2048,1024]{1,0:T(8,128)(2,1)S(1)}, bf16[2048,1024]{1,0:T(8,128)(2,1)}, u32[]{:S(2)}) copy-start(bf16[2048,1024]{1,0:T(8,128)(2,1)} %get-tuple-element.7) | copy-start | bytes 12582916
  121.6 2.0 %copy-start.1 = (bf16[768,512]{1,0:T(8,128)(2,1)S(1)}, bf16[768,512]{1,0:T(8,128)(2,1)}, u32[]{:S(2)}) copy-start(bf16[768,512]{1,0:T(8,128)(2,1)} %get-tuple-element.8) | copy-start | bytes 2359300

commit v2 on v1

--- a/solution.py
+++ b/solution.py
@@ -34,10 +34,10 @@
     return (serve_up, serve_down, mixed)
 
 
-def kernel(line, pieces, tok, gain, up, down, out_up, out_down, mixed,
-           wu, wd, xt, xn, act, part, pbuf, psum, rin_p, rin_y,
+def kernel(line, pieces, tok, gain, up, down_hbm, wu, wd, mixed,
+           xt, xn, act, part, pbuf, psum, rin_p, rin_y,
            w_send, w_recv, t_send, t_recv, a_send, a_recv, b_send, b_recv, c_send, c_recv,
-           o_sem, l_sem):
+           o_sem, l_sem, down, d_sem):
     T, dl = tok.shape
     r, F = up.shape
     D = wu.shape[0]
@@ -55,6 +55,11 @@
     half = T // 2
     zdev = ((fs + 2, tp), (fs - 2, tp), (fs + 1 - 2 * x, tp))
 
+    own_tok = pltpu.make_async_copy(tok, xt.at[tp], l_sem)
+    own_tok.start()
+    own_down = pltpu.make_async_copy(down_hbm, down, d_sem)
+    own_down.start()
+
     barrier = pltpu.get_barrier_semaphore()
 
     def greet(dev):
@@ -73,9 +78,6 @@
         for c in range(F // LANES):
             cols = slice(c * LANES, (c + 1) * LANES)
             wu[pl.ds(base + i * LANES, LANES), cols] = (g * up[rows, cols]).astype(jnp.bfloat16)
-    wd[pl.ds(base, r), :] = down[...].astype(jnp.bfloat16)
-    own_tok = pltpu.make_async_copy(tok, xt.at[tp], l_sem)
-    own_tok.start()
     links = 4 + has_up.astype(jnp.int32) + has_dn.astype(jnp.int32)
     pl.semaphore_wait(barrier, links)
 
@@ -121,45 +123,49 @@
     def place(idx):
         got = jnp.int32(0)
         for i in range(line):
-            order = sorted(range(line), key=lambda k: (abs(k - i), k if i < line / 2 else -k))
+            order = sorted(range(line), key=lambda k: (abs(k - i), -k if i < line / 2 else k))
             for q in range(line):
                 got = got + jnp.where((z == i) & (idx == q), jnp.int32(order[q]), jnp.int32(0))
         return got
 
-    def relay(a, idx, do, wait):
+    def relay(a, idx, do, wait, early=True, late=True):
         zz = place(idx)
         onward_up = (zz < z) & has_up
         onward_dn = (zz > z) & has_dn
         same, cross_s = zz * 2 + x, zz * 2 + 1 - x
         for p in one:
+            if not (early if pieces[p][0] < LANES else late):
+                continue
             if wait:
                 piece(a, same, p, 2).wait_recv()
             pl.when(onward_up)(lambda: do(piece(a, same, p, 0)))
             pl.when(onward_dn)(lambda: do(piece(a, same, p, 1)))
             do(piece(a, same, p, 2))
-        for p in two:
+        for p in two if late else ():
             for s in (same, cross_s):
                 if wait:
                     piece(a, s, p, 2).wait_recv()
                 pl.when(onward_up)(lambda: do(piece(a, s, p, 0)))
                 pl.when(onward_dn)(lambda: do(piece(a, s, p, 1)))
 
-    tok_copy(tok, tp, 0, mirror).start()
     own_x(0, start)
     own_z(0, start)
-    tok_copy(tok, tp, 1, partner).start()
+    own_tok.wait()
+    tok_copy(xt.at[tp], tp, 0, mirror).start()
+    tok_copy(xt.at[tp], tp, 1, partner).start()
+    own_down.wait()
+    wd[pl.ds(base, r), :] = down[...].astype(jnp.bfloat16)
     cross(0, start, True)
     for idx in range(1, line):
         relay(0, jnp.int32(idx), start, True)
         if idx == 1:
-            tok_copy(tok, mirror, 0, mirror).wait_recv()
+            tok_copy(xt.at[mirror], mirror, 0, mirror).wait_recv()
             tok_copy(xt.at[mirror], mirror, 2, partner).start()
     own_z(1, start)
     own_x(1, start)
 
-    own_tok.wait()
-    tok_copy(tok, partner, 1, partner).wait_recv()
-    tok_copy(tok, diag, 1, partner).wait_recv()
+    tok_copy(xt.at[partner], partner, 1, partner).wait_recv()
+    tok_copy(xt.at[diag], diag, 1, partner).wait_recv()
     block = 64
 
     def norm(i, carry):
@@ -180,10 +186,8 @@
         s = place(jnp.int32(idx)) * 2 + 1 - x
         for p in one:
             piece(0, s, p, 2).wait_recv()
-    up_out = pltpu.make_async_copy(wu, out_up, o_sem.at[line])
-    up_out.start()
-
-    mrows = LANES
+
+    mrows = 2 * LANES
 
     def first(i, carry):
         rows = pl.ds(pl.multiple_of(i * mrows, mrows), mrows)
@@ -193,7 +197,6 @@
         return carry
 
     lax.fori_loop(0, T // mrows, first, 0)
-    relay(1, jnp.int32(1), start, True)
 
     scale = (F * 4) ** (-0.5)
     mine = pl.ds(pl.multiple_of(core * half, half), half)
@@ -235,16 +238,16 @@
                        + pbuf[b].astype(jnp.float32)).astype(jnp.bfloat16)
             to_owner(b, o).start()
 
-    def out_copy(idx):
-        rows = pl.ds(pl.multiple_of(place(idx) * 2 * r, 2 * r), 2 * r)
-        return pltpu.make_async_copy(wd.at[rows, :], out_down.at[rows, :], o_sem.at[idx])
-
     def body(n, carry):
         idx, j = n // steps, n % steps
 
-        @pl.when((j == 0) & (idx >= 1) & (idx + 1 < line))
-        def _():
-            relay(1, idx + 1, start, True)
+        @pl.when((j == per) & (idx + 1 < line))
+        def _():
+            relay(1, idx + 1, start, True, late=False)
+
+        @pl.when((j == 1) & (idx >= 1))
+        def _():
+            relay(1, idx, start, True, early=False)
 
         far = place(idx) * 2 + 1 - x
         for h in range(per):
@@ -268,10 +271,6 @@
         def _():
             swap(b).start()
 
-        @pl.when(j == steps - 1)
-        def _():
-            out_copy(idx).start()
-
         @pl.when(n > 0)
         def _():
             second_half(block_of(n - 1))
@@ -323,13 +322,6 @@
         return carry
 
     lax.fori_loop(0, D // LANES, drain_sums, 0)
-    up_out.wait()
-
-    def drain_out(idx, carry):
-        out_copy(idx).wait()
-        return carry
-
-    lax.fori_loop(0, line, drain_out, 0)
 
 
 def cut(r):
@@ -357,12 +349,10 @@
     hbm = pl.BlockSpec(memory_space=pl.ANY)
     return pl.pallas_call(
         functools.partial(kernel, line, pieces),
-        out_shape=(jax.ShapeDtypeStruct((D, F), bf), jax.ShapeDtypeStruct((D, F), bf),
-                   jax.ShapeDtypeStruct((T, dl), bf)),
-        in_specs=[vmem] * 4,
-        out_specs=(hbm, hbm, vmem),
+        out_shape=(pltpu.VMEM((D, F), bf), pltpu.VMEM((D, F), bf), pltpu.VMEM((T, dl), bf)),
+        in_specs=[hbm, vmem, vmem, hbm],
+        out_specs=(vmem, vmem, vmem),
         scratch_shapes=[
-            pltpu.VMEM((D, F), bf), pltpu.VMEM((D, F), bf),
             pltpu.VMEM((4, T, dl), bf), pltpu.VMEM((T, D), bf), pltpu.VMEM((T, F), bf),
             pltpu.VMEM((nblk, T, LANES), bf), pltpu.VMEM((nblk, half, LANES), bf),
             pltpu.VMEM((nblk, half, LANES), bf),
@@ -371,9 +361,10 @@
             dma((3,)), dma((4,)),
             dma((nblk,)), dma((nb,)), dma((nblk,)), dma((nblk,)), dma((nblk,)), dma((nb, 2)),
             dma((line + 1,)), dma,
+            pltpu.VMEM((r, F), jnp.float32), dma,
         ],
         compiler_params=pltpu.CompilerParams(
-            collective_id=0, has_side_effects=True, vmem_limit_bytes=56 * 2 ** 20),
+            collective_id=0, has_side_effects=True, vmem_limit_bytes=55 * 2 ** 20),
     )(prompt_tokens, norm_gain.reshape(1, r), up_master, down_master)
 
 

time: 126 us -> 105 us (0.83); the launches traced: 124 us -> 105 us
  Pallas kernels: 116 us -> 99.3 us
  local copies, waits for them, and re-layouts: 7.72 us -> 4.91 us
    pallas_call x1, Pallas kernels: 116 us -> 99.3 us  [fused(): pl.pallas_call(functools.partial(kernel, line, pieces), out_shape=(pltpu....]
    unnamed x7 -> x3, local copies, waits for them, and re-layouts: 7.72 us -> 4.91 us
where the time goes in v2:
time: 105 us
  Pallas kernels  99.3 us (95%)
  local copies, waits for them, and re-layouts  4.91 us (5%)
    pallas_call x1, Pallas kernels, fused(): pl.pallas_call(functools.partial(kernel, line, pieces), out_shape=(pltpu....  99.3 us
    unnamed x3, local copies, waits for them, and re-layouts  4.91 us

profile of v2, /device:TPU:7, one launch (start us, length us, event | category | flops | bytes accessed | tf_op | source)
XLA Modules:
  0.0 104.9 jit_solution(8139797277761596910)
XLA Ops:
  0.6 99.3 %shard_map.67 = (bf16[2048,1024]{1,0:T(8,128)(2,1)S(1)}, bf16[2048,1024]{1,0:T(8,128)(2,1)S(1)}, bf16[768,512]{1,0:T(8,128)(2,1)S(1)}) custom-call(bf16[768,512]{1,0:T(8,128)(2,1)} %tok.1, f32[1,256]{1,0:T(1,128)} %bitcast.1, f32[256,1024]{1,0:T(8,128)} %up.1, f32[256,1024]{1,0:T(8,128)} %down_hbm.1), custom_call_target="tpu_custom_call" | custom-call | tf_op jit(solution)/shard_map/pallas_call | solution.py:350
  99.9 2.0 %copy.10 = bf16[2048,1024]{1,0:T(8,128)(2,1)} copy(bf16[2048,1024]{1,0:T(8,128)(2,1)S(1)} %get-tuple-element.3) | data formatting | bytes 8388608
  102.0 0.9 copy.12
  102.8 2.0 %copy.11 = bf16[2048,1024]{1,0:T(8,128)(2,1)} copy(bf16[2048,1024]{1,0:T(8,128)(2,1)S(1)} %get-tuple-element.4) | data formatting | bytes 8388608

commit v3 on v2

--- a/solution.py
+++ b/solution.py
@@ -83,7 +83,7 @@
 
     def piece(a, s, p, way):
         start, size = pieces[p][0], pieces[p][1]
-        ref = W[a].at[pl.ds(pl.multiple_of(s * r + start, 16), size), :]
+        ref = W[a].at[pl.ds(pl.multiple_of(s * r + start, 8), size), :]
         return pltpu.make_async_remote_copy(
             src_ref=ref, dst_ref=ref, send_sem=w_send.at[way, a, s, p],
             recv_sem=w_recv.at[a, s, p], device_id=zdev[way], device_id_type=MESH)
@@ -202,12 +202,17 @@
     mine = pl.ds(pl.multiple_of(core * half, half), half)
     theirs = pl.ds(pl.multiple_of((1 - core) * half, half), half)
     steps = 2 * per
+    inner = has_up & has_dn
+
+    def turn(n):
+        idx, j = n // steps, n % steps
+        last = idx == line - 1
+        return jnp.where(last, j % 2, j // per), jnp.where(last, j // 2, j % per)
 
     def block_of(n):
-        zz, j = place(n // steps), n % steps
-        side = j // per
-        s = zz * 2 + x + side * (1 - 2 * x)
-        return s * per + j % per
+        side, h = turn(n)
+        s = place(n // steps) * 2 + x + side * (1 - 2 * x)
+        return s * per + h
 
     def owner_of(b):
         o = b // nb
@@ -245,13 +250,18 @@
         def _():
             relay(1, idx + 1, start, True, late=False)
 
-        @pl.when((j == 1) & (idx >= 1))
+        @pl.when((j == per) & (idx + 1 < line) & (inner | (idx + 2 < line)))
+        def _():
+            relay(1, idx + 1, start, True, early=False)
+
+        @pl.when((j == steps - 2) & (idx == line - 1) & jnp.logical_not(inner))
         def _():
             relay(1, idx, start, True, early=False)
 
+        side, at = turn(n)
         far = place(idx) * 2 + 1 - x
         for h in range(per):
-            @pl.when(j == per + h)
+            @pl.when((side == 1) & (at == h))
             def _():
                 for p in one:
                     if pieces[p][0] // LANES == h:
@@ -325,7 +335,7 @@
 
 
 def cut(r):
-    across = min(LANES - 16, max(16, (r * 3 // 16) // 16 * 16))
+    across = min(LANES - 16, max(16, r * 5 // 32 // 8 * 8))
     got = []
     for first in range(0, r, LANES):
         rows = LANES if first + LANES < r else LANES - across
@@ -368,6 +378,33 @@
     )(prompt_tokens, norm_gain.reshape(1, r), up_master, down_master)
 
 
+def put(src_a, src_b, src_c, dst_a, dst_b, dst_c, sem):
+    copies = []
+    for src, dst in ((src_a, dst_a), (src_b, dst_b), (src_c, dst_c)):
+        n = 4 if src is not src_c else 1
+        rows = src.shape[0] // n
+        for i in range(n):
+            part = pl.ds(i * rows, rows)
+            copies.append(pltpu.make_async_copy(
+                src.at[part, :], dst.at[part, :], sem.at[len(copies)]))
+    for c in copies:
+        c.start()
+    for c in copies:
+        c.wait()
+
+
+def written(*arrays):
+    hbm = pl.BlockSpec(memory_space=pl.ANY)
+    return pl.pallas_call(
+        put,
+        out_shape=tuple(pltpu.HBM(a.shape, a.dtype) for a in arrays),
+        in_specs=[pl.BlockSpec(memory_space=pltpu.VMEM)] * 3,
+        out_specs=(pl.BlockSpec(memory_space=pltpu.HBM),) * 3,
+        scratch_shapes=[pltpu.SemaphoreType.DMA((9,))],
+        compiler_params=pltpu.CompilerParams(vmem_limit_bytes=2 ** 20),
+    )(*(pltpu.with_memory_space_constraint(a, pltpu.VMEM) for a in arrays))
+
+
 def solution(mesh):
     n_fs, n_tp = mesh.shape["fs"], mesh.shape["tp"]
 
@@ -378,7 +415,7 @@
                 and dl % LANES == 0 and T % (2 * LANES) == 0 and r * n_fs == dl * n_tp)
         if not fits:
             return plain(prompt_tokens, norm_gain, up_master, down_master)
-        return fused(n_fs, prompt_tokens, norm_gain, up_master, down_master)
+        return written(*fused(n_fs, prompt_tokens, norm_gain, up_master, down_master))
 
     return jax.shard_map(
         shards,

time: 105 us -> 102 us (0.971)
  local copies, waits for them, and re-layouts: 4.91 us -> 0 us
  Pallas kernels: 99.3 us -> 101 us
    unnamed x3 -> x0, local copies, waits for them, and re-layouts: 4.91 us -> none
    pallas_call x0 -> x1, Pallas kernels: none -> 3.6 us  [written(): pl.pallas_call(put, out_shape=tuple((pltpu.HBM(a.shape, a.dtype) for a in...]
    pallas_call x1, Pallas kernels: 99.3 us -> 97.4 us  [fused(): pl.pallas_call(functools.partial(kernel, line, pieces), out_shape=(pltpu....]
where the time goes in v3:
time: 102 us
  Pallas kernels  101 us (99%)
    pallas_call x1, Pallas kernels, fused(): pl.pallas_call(functools.partial(kernel, line, pieces), out_shape=(pltpu....  97.4 us
    pallas_call x1, Pallas kernels, written(): pl.pallas_call(put, out_shape=tuple((pltpu.HBM(a.shape, a.dtype) for a in...  3.6 us

profile of v3, /device:TPU:7, one launch (start us, length us, event | category | flops | bytes accessed | tf_op | source)
XLA Modules:
  0.0 101.7 jit_solution(8824948665410367491)
XLA Ops:
  0.6 97.4 %shard_map.67 = (bf16[2048,1024]{1,0:T(8,128)(2,1)S(1)}, bf16[2048,1024]{1,0:T(8,128)(2,1)S(1)}, bf16[768,512]{1,0:T(8,128)(2,1)S(1)}) custom-call(bf16[768,512]{1,0:T(8,128)(2,1)} %tok.1, f32[1,256]{1,0:T(1,128)} %bitcast.1, f32[256,1024]{1,0:T(8,128)} %up.1, f32[256,1024]{1,0:T(8,128)} %down_hbm.1), custom_call_target="tpu_custom_call" | custom-call | tf_op jit(solution)/shard_map/pallas_call | solution.py:360
  98.1 3.6 %shard_map.68 = (bf16[2048,1024]{1,0:T(8,128)(2,1)}, bf16[2048,1024]{1,0:T(8,128)(2,1)}, bf16[768,512]{1,0:T(8,128)(2,1)}) custom-call(bf16[2048,1024]{1,0:T(8,128)(2,1)S(1)} %get-tuple-element.6.src_a, bf16[2048,1024]{1,0:T(8,128)(2,1)S(1)} %get-tuple-element.7.src_b, bf16[768,512]{1,0:T(8,128)(2,1)S(1)} %get-tuple-element.8.src_c), custom_call_target="tpu_custom_call" | custom-call | tf_op jit(solution)/shard_map/pallas_call | solution.py:398
